TPU v7x, 32 devices: a whole 2x2x4 slice. The times are simulated.
32 devices in a mesh: sp: 8 (over z, y), tp: 4 (over x, core).
Axes of the slice: x: 2, y: 2, z: 4, core: 2. Of those that a mesh axis runs over, the one named last changes fastest.
Arguments:
- prompt: bfloat16 [4, 1536, 4096], P(None, 'sp'), may hold values from -6 to 6
- forget_weight: bfloat16 [4096, 2048], P(None, 'tp'), may hold values from -0.09375 to 0.09375
- value_weight: bfloat16 [4096, 2048], P(None, 'tp'), may hold values from -1.5 to 1.5
- lower_bound: float32 [2048], P('tp'), may hold values from 0.9 to 0.9996745
- extra_decay: float32 [4, 1536, 2048], P(None, 'sp', 'tp'), may hold values from -1.4045573 to 0
- new_token: bfloat16 [4, 4096], P(None, 'tp'), may hold values from -6 to 6
- new_query: bfloat16 [4, 2048], P(None, 'tp'), may hold values from -6 to 6
- read_gain: float32 [128], replicated, may hold values from 0.1 to 1.9
Outputs:
- state_cache: bfloat16 [128, 16, 4, 128], P('sp', 'tp')
- first_read: bfloat16 [4, 2048], P(None, 'tp')
All inputs are finite; a program needn't handle non-finite values.
Results may differ from a plain program's by a relative error of at most 0.0019.
The roundings to bfloat16 on the way count: a program that leaves them out, or rounds other values in their place, can miss the bound.
Values may be sent and summed in bfloat16 or wider, within the bound.
A program may use at most 64 MiB of HBM per device.

v0:
```python
import jax
import jax.numpy as jnp
from jax import lax
from jax.sharding import PartitionSpec as P

HD = 128


def entering(value, axis, join, neutral):
    count, mine = (lax.axis_size(axis), lax.axis_index(axis))
    pieces = lax.all_gather(value, axis)
    pieces = pieces[::-1]
    mine = count - 1 - mine
    total = jnp.full_like(value, 0) + jnp.asarray(neutral, value.dtype)

    def hop(position, total):
        longer = join(total, pieces[position])
        return jnp.where(position < mine, longer, total)

    return lax.fori_loop(0, count - 1, hop, total)


def add_terms(earlier, latter):
    return earlier + latter


def read_share(state_rows, decay_rows, key_share, query_rows, new_value):
    updated = jnp.exp(decay_rows)[..., None] * state_rows + key_share[..., None] * new_value[None]
    return jnp.sum(query_rows[..., None] * updated, axis=0)


def local(
    prompt, forget_weight, value_weight, lower_bound, extra_decay, new_token, new_query, read_gain
):
    seq_count = prompt.shape[0]
    span_len = prompt.shape[1]
    width_dev = forget_weight.shape[1]
    head_count = width_dev // HD
    log_lower = jnp.log(lower_bound)
    log_upper = jnp.log1p(-lower_bound)
    opening = 1.0 - lower_bound
    forget_pre = jnp.einsum(
        "std,dw->stw", prompt, forget_weight, preferred_element_type=jnp.float32
    ).astype(jnp.bfloat16)
    values = jnp.einsum(
        "std,dw->stw", prompt, value_weight, preferred_element_type=jnp.float32
    ).astype(jnp.bfloat16)
    forget_wide = lax.optimization_barrier(forget_pre).astype(jnp.float32)
    log_forget = jnp.logaddexp(log_lower, log_upper + jax.nn.log_sigmoid(forget_wide)) + extra_decay
    key_rows = opening * jax.nn.sigmoid(-forget_wide)
    running = jnp.cumsum(log_forget, axis=1)
    totals = running[:, -1]
    weighted = (key_rows * jnp.exp(totals[:, None] - running)).astype(jnp.bfloat16)
    weighted = weighted.reshape(seq_count, span_len, head_count, HD)
    value_rows = values.reshape(seq_count, span_len, head_count, HD)
    later_sum = entering(totals, "sp", add_terms, jnp.zeros_like(totals))
    end_scale = jnp.exp(later_sum).reshape(seq_count, head_count, HD).transpose(2, 1, 0)
    whole_token = lax.all_gather(new_token, "tp", axis=1, tiled=True)
    new_forget = lax.optimization_barrier(
        jnp.dot(whole_token, forget_weight, preferred_element_type=jnp.float32).astype(jnp.bfloat16)
    ).astype(jnp.float32)
    new_value = lax.optimization_barrier(
        jnp.dot(whole_token, value_weight, preferred_element_type=jnp.float32).astype(jnp.bfloat16)
    ).astype(jnp.float32)
    new_log = jnp.logaddexp(log_lower, log_upper + jax.nn.log_sigmoid(new_forget))
    new_key = opening * jax.nn.sigmoid(-new_forget)
    query_act = jax.nn.silu(new_query.astype(jnp.float32))
    decay_cols = new_log.reshape(seq_count, head_count, HD).transpose(2, 1, 0)
    key_cols = new_key.reshape(seq_count, head_count, HD).transpose(2, 1, 0)
    query_cols = query_act.reshape(seq_count, head_count, HD).transpose(2, 1, 0)
    value_cols = new_value.reshape(seq_count, head_count, HD).transpose(1, 0, 2)
    row_share = HD // lax.axis_size("sp")
    first_own = lax.axis_index("sp") * row_share
    block_state = jnp.einsum(
        "sthd,sthe->dhse", weighted, value_rows, preferred_element_type=jnp.float32
    )
    whole_state = lax.psum(block_state * end_scale[..., None], "sp")
    state_cache = lax.dynamic_slice_in_dim(whole_state, first_own, row_share, 0).astype(
        jnp.bfloat16
    )
    raw_read = read_share(whole_state, decay_cols, key_cols, query_cols, value_cols)
    raw_read = raw_read.transpose(1, 0, 2)
    normed = (
        raw_read
        * lax.rsqrt(jnp.mean(raw_read * raw_read, axis=-1, keepdims=True) + 1e-06)
        * read_gain
    )
    first_read = normed.reshape(seq_count, width_dev).astype(jnp.bfloat16)
    return (state_cache, first_read)


def solution(mesh):
    return jax.shard_map(
        local,
        mesh=mesh,
        in_specs=(
            P(None, "sp", None),
            P(None, "tp"),
            P(None, "tp"),
            P("tp"),
            P(None, "sp", "tp"),
            P(None, "tp"),
            P(None, "tp"),
            P(),
        ),
        out_specs=(P("sp", "tp", None, None), P(None, "tp")),
        check_vma=False,
    )
```

profile of v0, /device:TPU:0, one launch (start us, length us, event | category | flops | bytes accessed | tf_op | source)
XLA Modules:
  0.0 154.1 jit_solution(2838277091920605518)
XLA Ops:
  7.2 0.0 all-reduce.3.cloned.1.call-start
  7.2 0.7 broadcast_subtract_fusion
  7.9 0.0 copy-start.1
  7.9 7.5 %fusion.23 = bf16[4,192,512]{2,1,0:T(8,128)(2,1)S(1)} fusion(bf16[4,192,4096]{2,1,0:T(8,128)(2,1)} %param.10, bf16[4096,512]{1,0:T(8,128)(2,1)} %param.11), kind=kOutput, calls=%fused_computation.27 | convolution fusion | flops 3221618688 | bytes 11272192 | tf_op jit(solution)/shard_map/std,dw->stw/dot_general | solution.py:42
  15.4 0.0 copy-done.1
  15.5 2.0 %add_bitcast_fusion = f32[4,512,192]{1,2,0:T(8,128)S(1)} fusion(f32[4,192,512]{2,1,0:T(8,128)S(1)} %copy-done.1, bf16[4,192,512]{2,1,0:T(8,128)(2,1)S(1)} %fusion.23, f32[512]{0:T(512)S(1)} %get-tuple-element.112, f32[512]{0:T(512)S(1)} %get-tuple-element.113), kind=kLoop, calls=%fused_computation.24 | loop fusion | flops 7471104 | bytes 3936256 | tf_op jit(solution)/shard_map/transpose
  17.4 0.2 pad.3
  17.7 1.6 %fusion.4 = f32[4,512,2,128]{1,2,3,0:T(2,128)S(1)} fusion(f32[4,512,2,128]{1,3,2,0:T(8,128)S(1)} %bitcast.83), kind=kOutput, calls=%fused_computation.6 | output fusion | flops 66584576 | bytes 4194304 | tf_op jit(solution)/shard_map/reduce-window
  19.3 0.1 reduce-window.9
  19.4 0.7 broadcast_add_fusion
  20.1 0.4 copy.21
  20.6 32.4 %all-gather = f32[32,1,512]{2,1,0:T(1,128)S(1)} all-gather(f32[4,1,512]{2,1,0:T(1,128)S(1)} %slice.19), channel_id=2, replica_groups=mesh['sp'=8,'tp'=4] {'sp'}, dimensions={0}, use_global_device_ids=true | all-gather | bytes 73728 | tf_op jit(solution)/shard_map/all_gather | solution.py:11
  52.9 0.2 reduce
  53.1 0.3 while.14
  53.4 7.4 %fusion.27 = bf16[4,24,4,8,128]{4,3,2,1,0:T(8,128)(2,1)S(1)} fusion(bf16[4,192,4096]{2,1,0:T(8,128)(2,1)} %param.10, bf16[4096,512]{1,0:T(8,128)(2,1)} %param.12), kind=kOutput, calls=%fused_computation.30 | convolution fusion | flops 3221618688 | bytes 11272192 | tf_op jit(solution)/shard_map/std,dw->stw/dot_general | solution.py:45
  60.9 0.0 copy-start.2
  60.9 2.0 %fusion.26 = f32[128,4,4,128]{0,3,2,1:T(8,128)} fusion(bf16[4,24,4,8,128]{4,3,2,1,0:T(8,128)(2,1)S(1)} %fusion.27, f32[128,4,4]{0,2,1:T(4,128)S(1)} %exponential_bitcast_fusion.1, f32[4,256,512]{2,1,0:T(8,128)S(1)} %bitcast.85, f32[4,512]{1,0:T(4,128)S(1)} %bitcast.86, bf16[4,192,512]{2,1,0:T(8,128)(2,1)S(1)} %fusion.23, f32[512]{0:T(512)S(1)} %get-tuple-element.111), kind=kOutput, calls=%fused_computation.29 | convolution fusion | flops 103677952 | bytes 4212736 | tf_op jit(solution)/shard_map/sthd,sthe->dhse/dot_general | solution.py:74
  62.9 0.0 all-reduce.3.cloned.1.call-update
  62.9 0.0 copy-done.2
  62.9 5.2 %all_gather.7 = bf16[4,4096]{1,0:T(4,128)(2,1)S(1)} all-gather(bf16[4,1024]{1,0:T(4,128)(2,1)S(1)} %copy-done.2), channel_id=1, replica_groups=mesh['sp'=8,'tp'=4] {'tp'}, dimensions={1}, use_global_device_ids=true | all-gather | bytes 40960 | tf_op jit(solution)/shard_map/all_gather | solution.py:58
  68.1 3.2 %convolution_convert_fusion.1 = bf16[4,512]{1,0:T(4,128)(2,1)S(1)} fusion(bf16[4,4096]{1,0:T(4,128)(2,1)S(1)} %all_gather.7, bf16[4096,512]{1,0:T(8,128)(2,1)} %param.11), kind=kOutput, calls=%fused_computation.32 | convolution fusion | flops 16779264 | bytes 4231168 | tf_op jit(solution)/shard_map/dot_general | solution.py:60
  71.4 0.5 copy-done
  71.8 0.6 convolution_convert_fusion
  72.5 0.0 copy-done.3
  72.5 0.1 exponential_bitcast_fusion
  72.6 69.7 %all-reduce.3.cloned.1.call-done = f32[128,4,4,128]{0,3,2,1:T(8,128)} async-done(((f32[128,4,4,128]{0,3,2,1:T(8,128)}), f32[128,4,4,128]{0,3,2,1:T(8,128)}) %all-reduce.3.cloned.1.call-update) | async-done | bytes 1048592 | tf_op jit(solution)/shard_map/psum | solution.py:77
  142.3 1.9 %multiply_reduce_fusion = f32[4,4,128]{2,1,0:T(4,128)S(1)} fusion(f32[128,4,4,128]{0,3,2,1:T(8,128)} %all-reduce.3.cloned.1.call-done, f32[4,4,128]{2,1,0:T(4,128)S(1)} %convert_bitcast_fusion, f32[128,4,4]{0,2,1:T(4,128)S(1)} %get-tuple-element.110, f32[128,4,4]{0,2,1:T(4,128)S(1)} %get-tuple-element.109, f32[128,4,4]{0,2,1:T(4,128)S(1)} %get-tuple-element.114), kind=kLoop, calls=%fused_computation.33 | loop fusion | flops 1308672 | bytes 1089536 | tf_op jit(solution)/shard_map/reduce_sum | solution.py:29
  144.2 0.1 fusion.50
  144.3 1.4 dynamic-slice_convert_fusion
  145.7 0.8 copy.29
  146.6 0.0 copy-done.4
  146.6 0.7 fusion.53
  (20 shorter events, 0.2 us)
Async XLA Ops:
  7.2 135.2 %all-reduce.3.cloned.1.call-start = ((), (), s32[]{:S(2)}) async-start(), calls=%async_computation | async-start | bytes 2097152 | tf_op jit(solution)/shard_map/psum | solution.py:77
  7.9 7.5 %copy-start.1 = (f32[4,192,512]{2,1,0:T(8,128)S(1)}, f32[4,192,512]{2,1,0:T(8,128)}, u32[]{:S(2)}) copy-start(f32[4,192,512]{2,1,0:T(8,128)} %param.14) | copy-start | bytes 4718596
  60.9 2.1 %copy-start.2 = (bf16[4,1024]{1,0:T(4,128)(2,1)S(1)}, bf16[4,1024]{1,0:T(4,128)(2,1)}, u32[]{:S(2)}) copy-start(bf16[4,1024]{1,0:T(4,128)(2,1)} %param.15) | copy-start | bytes 24580
  68.1 3.7 %copy-start = (bf16[4096,512]{1,0:T(8,128)(2,1)S(1)}, bf16[4096,512]{1,0:T(8,128)(2,1)}, u32[]{:S(2)}) copy-start(bf16[4096,512]{1,0:T(8,128)(2,1)} %param.12) | copy-start | bytes 12582916
  71.8 0.7 copy-start.3
  72.5 74.1 %copy-start.4 = (f32[128]{0:T(128)S(1)}, f32[128]{0:T(128)}, u32[]{:S(2)}) copy-start(f32[128]{0:T(128)} %param.17) | copy-start | bytes 1540
Sparse Core Ops, SparseCore 0:
  63.0 79.2 all-reduce.2
where the time goes:
time: 154 us
  waiting for transfers between devices  69.8 us (45%)
  blocking collectives  37.5 us (24%)
  matrix products  20.8 us (14%)
  between operations  14.2 us (9%)
  other arithmetic  8.07 us (5%)
  local copies, waits for them, and re-layouts  3.48 us (2%)
    psum x1, waiting for transfers between devices, local(): whole_state = lax.psum(block_state * end_scale[..., None], 'sp')  69.7 us
    all_gather x1, blocking collectives, entering(): pieces = lax.all_gather(value, axis)  32.4 us
    dot_general x1, matrix products, local(): jnp.einsum('std,dw->stw', prompt, forget_weight, preferred_element_type=j...  7.52 us
    dot_general x1, matrix products, local(): jnp.einsum('std,dw->stw', prompt, value_weight, preferred_element_type=jn...  7.42 us
    all_gather x1, blocking collectives, local(): whole_token = lax.all_gather(new_token, 'tp', axis=1, tiled=True)  5.19 us
    dot_general x1, matrix products, local(): jnp.dot(whole_token, forget_weight, preferred_element_type=jnp.float32)  3.23 us
  transfers between devices with their start and end apart: 1, of which 1 were waited for; matrix products, arithmetic and copies ran while one was open for 3% of the time, Pallas kernels for 0%

commit v1 on v0

v1 whole, which is shorter than its diff:
```python
import functools

import jax
import jax.numpy as jnp
from jax import lax
from jax.experimental import pallas as pl
from jax.experimental.pallas import tpu as pltpu
from jax.sharding import PartitionSpec as P

HD = 128
PAD = 16
CHUNKS = 4
MESH = pl.DeviceIdType.MESH
F32 = jnp.float32
BF16 = jnp.bfloat16


def near_size(count):
    near = 1
    while near * near * 4 <= count:
        near *= 2
    return near


def kernel(
    n, m, near,
    prompt, forget_w, value_w, lower, extra, token, query, gain,
    state_out, read_out,
    xs, ws, ex, acc, toks, bs, ry, pz, rz, tb, rp, lcol, qk, kv,
    x_sem, w_sem, e_sem, tok_send, tok_recv, t_send, t_recv, y_send, y_recv,
    z_send, z_recv, r_send, r_recv,
):
    far = n // near
    seqs, span, depth = prompt.shape
    rows = seqs * span
    heads = forget_w.shape[1] // HD
    share = HD // n
    kc = depth // CHUNKS
    tk = token.shape[1]
    me, mt = lax.axis_index("sp"), lax.axis_index("tp")
    my_far, my_near = me // near, me % near

    x_copies, w_copies = [], {}
    for c in range(CHUNKS):
        ks = pl.ds(c * kc, kc)
        part = []
        for s in range(seqs):
            cp = pltpu.make_async_copy(
                prompt.at[s, :, ks], xs.at[pl.ds(s * span, span), ks], x_sem.at[c, s]
            )
            cp.start()
            part.append(cp)
        x_copies.append(part)
        for i, w in enumerate((forget_w, value_w)):
            cp = pltpu.make_async_copy(
                w.at[ks, pl.ds(0, HD)], ws.at[0, ks, pl.ds(i * HD, HD)], w_sem.at[0, c, i]
            )
            cp.start()
            w_copies[0, c, i] = cp
    e_copy = pltpu.make_async_copy(extra, ex, e_sem)
    e_copy.start()
    for h in range(1, heads):
        for c in range(CHUNKS):
            ks = pl.ds(c * kc, kc)
            for i, w in enumerate((forget_w, value_w)):
                cp = pltpu.make_async_copy(
                    w.at[ks, pl.ds(h * HD, HD)],
                    ws.at[h, ks, pl.ds(i * HD, HD)],
                    w_sem.at[h, c, i],
                )
                cp.start()
                w_copies[h, c, i] = cp

    barrier = pltpu.get_barrier_semaphore()
    for k in range(1, m):
        pl.semaphore_signal(
            barrier, inc=1, device_id={"tp": lax.rem(mt + k, m)}, device_id_type=MESH
        )
    for k in range(1, n):
        pl.semaphore_signal(
            barrier, inc=1, device_id={"sp": lax.rem(me + k, n)}, device_id_type=MESH
        )
    pl.semaphore_wait(barrier, n + m - 2)

    sends = []

    def send(src, dst, s_sem, r_sem, target):
        cp = pltpu.make_async_remote_copy(
            src_ref=src, dst_ref=dst, send_sem=s_sem, recv_sem=r_sem,
            device_id=target, device_id_type=MESH,
        )
        cp.start()
        sends.append(cp)
        return cp

    tok_copies = [
        send(token, toks.at[mt], tok_send.at[k], tok_recv.at[k], {"tp": lax.rem(mt + k, m)})
        for k in range(1, m)
    ]
    toks[mt] = token[...]

    def lanes(ref, h):
        return ref[pl.ds(h * HD, HD)].reshape(1, HD)

    def matmul(h):
        tall = rows if h == 0 else rows + PAD
        for c in range(CHUNKS):
            if h == 0:
                for cp in x_copies[c]:
                    cp.wait()
            for i in range(2):
                w_copies[h, c, i].wait()
            ks = pl.ds(c * kc, kc)
            part = jnp.dot(xs[pl.ds(0, tall), ks], ws[h, ks, :], preferred_element_type=F32)
            if c == 0:
                acc[h % 2, pl.ds(0, tall), :] = part
            else:
                acc[h % 2, pl.ds(0, tall), :] += part

    t_copies, y_copies, z_copies = {}, {}, {}

    def gate(h):
        opening = 1.0 - lanes(lower, h)
        at = lax.broadcasted_iota(jnp.int32, (span, HD), 0)

        def later(x, k):
            if k % 8 == 0:
                return jnp.concatenate([x[k:], jnp.ones((k, HD), F32)], axis=0)
            return jnp.where(at < span - k, pltpu.roll(x, span - k, 0), 1.0)

        for s in range(seqs):
            block = pl.ds(s * span, span)
            pre = acc[h % 2, block, pl.ds(0, HD)].astype(BF16).astype(F32)
            values = acc[h % 2, block, pl.ds(HD, HD)].astype(BF16)
            key = opening / (1.0 + jnp.exp(pre))
            keep = (1.0 - key) * jnp.exp(ex[s, :, pl.ds(h * HD, HD)])
            after = later(keep, 1)
            k = 1
            while k < span:
                after = after * later(after, k)
                k *= 2
            weighted = (key * after).astype(BF16)
            tb[h, me, pl.ds(s, 1), :] = after[0:1] * keep[0:1]
            state = lax.dot_general(
                weighted, values, (((0,), (0,)), ((), ())), preferred_element_type=F32
            )
            for f in range(far):
                for y in range(near):
                    lo = (f * near + y) * share
                    bs[h, y, f, s] = state[lo : lo + share]
        t_copies[h] = [
            send(tb.at[h, me], tb.at[h, me], t_send.at[h, k], t_recv.at[h, k],
                 {"sp": lax.rem(me + k, n)})
            for k in range(1, n)
        ]
        y_copies[h] = []
        for k in range(1, near):
            y = lax.rem(my_near + k, near)
            y_copies[h].append(
                send(bs.at[h, y], ry.at[h, k - 1], y_send.at[h, k - 1], y_recv.at[h, k - 1],
                     {"sp": my_far * near + y})
            )

    def scale_after(h, block):
        total = jnp.ones((seqs, HD), F32)
        for b in range(n):
            total = total * jnp.where(b > block, tb[h, b], 1.0)
        return total

    def combine(h):
        for cp in t_copies[h]:
            cp.wait_recv()
        sources = [lax.rem(my_near + near - k, near) for k in range(near)]
        scales = [scale_after(h, my_far * near + y) for y in sources]
        fill = HD - near * seqs
        cols = jnp.concatenate(scales + [jnp.zeros((fill, HD), F32)], axis=0).T
        for f in range(far):
            for y in range(near):
                lo = (f * near + y) * share
                lcol[h, y, f] = cols[lo : lo + share]
        for cp in y_copies[h]:
            cp.wait_recv()
        for f in range(far):
            col = lcol[h, my_near, f]
            for s in range(seqs):
                total = bs[h, my_near, f, s] * col[:, s : s + 1]
                for k in range(1, near):
                    j = k * seqs + s
                    total += ry[h, k - 1, f, s] * col[:, j : j + 1]
                pz[h, f, s] = total
        z_copies[h] = []
        for k in range(1, far):
            f = lax.rem(my_far + k, far)
            z_copies[h].append(
                send(pz.at[h, f], rz.at[h, k - 1], z_send.at[h, k - 1], z_recv.at[h, k - 1],
                     {"sp": f * near + my_near})
            )

    def finish(h):
        for cp in z_copies[h]:
            cp.wait_recv()
        for s in range(seqs):
            total = pz[h, my_far, s]
            for k in range(1, far):
                total += rz[h, k - 1, s]
            state_out[h, s] = total.astype(BF16)

    def token_terms(h, block):
        new_pre = block[0:seqs, 0:HD].astype(BF16).astype(F32)
        new_value = block[0:seqs, HD : 2 * HD].astype(BF16).astype(F32)
        new_key = (1.0 - lanes(lower, h)) / (1.0 + jnp.exp(new_pre))
        q = query[:, pl.ds(h * HD, HD)].astype(F32)
        q = q / (1.0 + jnp.exp(-q))
        qk[h] = q * (1.0 - new_key)
        kv[h] = jnp.sum(q * new_key, axis=1, keepdims=True) * new_value

    def read_part(h):
        row = qk[h] * scale_after(h, me)
        col = jnp.concatenate([row, jnp.zeros((HD - seqs, HD), F32)], axis=0).T
        for s in range(seqs):
            total = jnp.zeros((share, HD), F32)
            for f in range(far):
                for y in range(near):
                    lo = (f * near + y) * share
                    total += bs[h, y, f, s] * col[lo : lo + share, s : s + 1]
            rp[me, h, pl.ds(s, 1), :] = jnp.sum(total, axis=0, keepdims=True)

    e_waited = False
    for h in range(heads):
        if h == 1:
            for cp in tok_copies:
                cp.wait_recv()
            xs[pl.ds(rows, PAD), :] = jnp.zeros((PAD, depth), BF16)
            for c in range(m):
                xs[pl.ds(rows, seqs), pl.ds(c * tk, tk)] = toks[c]
        matmul(h)
        if not e_waited:
            e_copy.wait()
            e_waited = True
        gate(h)
        if h >= 1:
            token_terms(h, acc[h % 2, pl.ds(rows, PAD), :])
            combine(h - 1)
        if h >= 2:
            finish(h - 2)
    first = jnp.dot(xs[pl.ds(rows, PAD), :], ws[0], preferred_element_type=F32)
    token_terms(0, first)
    for h in range(heads - 1):
        read_part(h)
    combine(heads - 1)
    read_part(heads - 1)
    r_copies = [
        send(rp.at[me], rp.at[me], r_send.at[k], r_recv.at[k], {"sp": lax.rem(me + k, n)})
        for k in range(1, n)
    ]
    if heads > 1:
        finish(heads - 2)
    for cp in r_copies:
        cp.wait_recv()
    for h in range(heads):
        raw = kv[h]
        for b in range(n):
            raw = raw + rp[b, h]
        mean = jnp.mean(raw * raw, axis=1, keepdims=True)
        normed = raw * lax.rsqrt(mean + 1e-6) * lanes(gain, 0)
        read_out[:, pl.ds(h * HD, HD)] = normed.astype(BF16)
    finish(heads - 1)
    for cp in sends:
        cp.wait_send()


def local(n, m, prompt, forget_w, value_w, lower, extra, token, query, gain):
    seqs, span, depth = prompt.shape
    rows = seqs * span
    width = forget_w.shape[1]
    heads = width // HD
    share = HD // n
    near = near_size(n)
    far = n // near
    vmem = pl.BlockSpec(memory_space=pltpu.VMEM)
    hbm = pl.BlockSpec(memory_space=pl.ANY)
    dma = pltpu.SemaphoreType.DMA
    state, read = pl.pallas_call(
        functools.partial(kernel, n, m, near),
        out_shape=(
            jax.ShapeDtypeStruct((heads, seqs, share, HD), BF16),
            jax.ShapeDtypeStruct((seqs, width), BF16),
        ),
        in_specs=[hbm, hbm, hbm, vmem, hbm, vmem, vmem, vmem],
        out_specs=(vmem, vmem),
        scratch_shapes=[
            pltpu.VMEM((rows + PAD, depth), BF16),
            pltpu.VMEM((heads, depth, 2 * HD), BF16),
            pltpu.VMEM((seqs, span, width), F32),
            pltpu.VMEM((2, rows + PAD, 2 * HD), F32),
            pltpu.VMEM((m, seqs, token.shape[1]), BF16),
            pltpu.VMEM((heads, near, far, seqs, share, HD), F32),
            pltpu.VMEM((heads, near - 1, far, seqs, share, HD), F32),
            pltpu.VMEM((heads, far, seqs, share, HD), F32),
            pltpu.VMEM((heads, far - 1, seqs, share, HD), F32),
            pltpu.VMEM((heads, n, seqs, HD), F32),
            pltpu.VMEM((n, heads, seqs, HD), F32),
            pltpu.VMEM((heads, near, far, share, HD), F32),
            pltpu.VMEM((heads, seqs, HD), F32),
            pltpu.VMEM((heads, seqs, HD), F32),
            dma((CHUNKS, seqs)),
            dma((heads, CHUNKS, 2)),
            dma,
            dma((m,)),
            dma((m,)),
            dma((heads, n)),
            dma((heads, n)),
            dma((heads, near - 1)),
            dma((heads, near - 1)),
            dma((heads, far - 1)),
            dma((heads, far - 1)),
            dma((n,)),
            dma((n,)),
        ],
        compiler_params=pltpu.CompilerParams(collective_id=0, has_side_effects=True),
    )(prompt, forget_w, value_w, lower, extra, token, query, gain)
    return state.transpose(2, 0, 1, 3), read


def solution(mesh):
    return jax.shard_map(
        functools.partial(local, mesh.shape["sp"], mesh.shape["tp"]),
        mesh=mesh,
        in_specs=(
            P(None, "sp", None),
            P(None, "tp"),
            P(None, "tp"),
            P("tp"),
            P(None, "sp", "tp"),
            P(None, "tp"),
            P(None, "tp"),
            P(),
        ),
        out_specs=(P("sp", "tp", None, None), P(None, "tp")),
        check_vma=False,
    )
```

time: 154 us -> 39.8 us (0.26)
  waiting for transfers between devices: 69.8 us -> 0 us
  blocking collectives: 37.5 us -> 0 us
  Pallas kernels: 0 us -> 36.1 us
  matrix products: 20.8 us -> 0 us
  between operations: 14.2 us -> 0.64 us
  other arithmetic: 8.07 us -> 0 us
    psum x1 -> x0, waiting for transfers between devices: 69.7 us -> none  [local(): whole_state = lax.psum(block_state * end_scale[..., None], 'sp')]
    all_gather x2 -> x0, blocking collectives: 37.5 us -> none  [the longest x1 32.4 us: entering(): pieces = lax.all_gather(value, axis)]
    pallas_call x0 -> x1, Pallas kernels: none -> 36.1 us  [local(): pl.pallas_call(functools.partial(kernel, n, m, near), out_shape=(jax.Shap...]
    dot_general x5 -> x0, matrix products: 20.8 us -> none  [the longest x1 7.52 us: local(): jnp.einsum('std,dw->stw', prompt, forget_weight, preferred_element_type=j...]
    another operation x3 -> x0, other arithmetic: 2.42 us -> none
    transpose x2 -> x0, other arithmetic: 2 us -> none
    reduce_sum x2 -> x0, other arithmetic: 1.95 us -> none  [the longest x1 1.86 us: read_share(): return jnp.sum(query_rows[..., None] * updated, axis=0)]
  transfers between devices with their start and end apart: 1 -> 0, of which waited for: 1 -> 0; matrix products, arithmetic and copies ran while one was open for 3% -> 0% of each run, Pallas kernels for 0% -> 0%
where the time goes in v1:
time: 39.8 us; the launch traced here: 39.5 us
  Pallas kernels  36.1 us (91%)
  local copies, waits for them, and re-layouts  2.77 us (7%)
  between operations  0.64 us (2%)
    pallas_call x1, Pallas kernels, local(): pl.pallas_call(functools.partial(kernel, n, m, near), out_shape=(jax.Shap...  36.1 us
    unnamed x2, local copies, waits for them, and re-layouts  2.77 us

profile of v1, /device:TPU:0, one launch (start us, length us, event | category | flops | bytes accessed | tf_op | source)
XLA Modules:
  0.0 39.5 jit_solution(8425471203037675335)
XLA Ops:
  0.6 36.1 %shard_map.95 = (bf16[4,4,16,128]{3,2,1,0:T(8,128)(2,1)}, bf16[4,512]{1,0:T(4,128)(2,1)}) custom-call(bf16[4,192,4096]{2,1,0:T(8,128)(2,1)} %prompt.1, bf16[4096,512]{1,0:T(8,128)(2,1)} %forget_w.1, bf16[4096,512]{1,0:T(8,128)(2,1)} %value_w.1, f32[512]{0:T(512)} %lower.1, f32[4,192,512]{2,1,0:T(8,128)} %extra.1, bf16[4,1024]{1,0:T(4,128)(2,1)} %token_.1, ...), custom_call_target="tpu_custom_call" | custom-call | tf_op jit(solution)/shard_map/pallas_call | solution.py:283
  36.7 1.5 %copy.10 = bf16[16,4,4,128]{3,2,1,0:T(4,128)(2,1)} copy(bf16[16,4,4,128]{3,0,2,1:T(8,128)(2,1)} %bitcast.1) | data formatting | bytes 131072
  38.2 1.3 %copy.12 = bf16[4,512]{1,0:T(4,128)(2,1)} copy(bf16[4,512]{1,0:T(4,128)(2,1)} %get-tuple-element.11) | data formatting | bytes 8192

commit v2 on v1

--- a/solution.py
+++ b/solution.py
@@ -10,6 +10,7 @@
 HD = 128
 PAD = 16
 CHUNKS = 4
+GROUP = 2
 MESH = pl.DeviceIdType.MESH
 F32 = jnp.float32
 BF16 = jnp.bfloat16
@@ -34,6 +35,7 @@
     seqs, span, depth = prompt.shape
     rows = seqs * span
     heads = forget_w.shape[1] // HD
+    groups, wide = heads // GROUP, GROUP * HD
     share = HD // n
     kc = depth // CHUNKS
     tk = token.shape[1]
@@ -53,23 +55,23 @@
         x_copies.append(part)
         for i, w in enumerate((forget_w, value_w)):
             cp = pltpu.make_async_copy(
-                w.at[ks, pl.ds(0, HD)], ws.at[0, ks, pl.ds(i * HD, HD)], w_sem.at[0, c, i]
+                w.at[ks, pl.ds(0, wide)], ws.at[0, ks, pl.ds(i * wide, wide)], w_sem.at[0, c, i]
             )
             cp.start()
             w_copies[0, c, i] = cp
     e_copy = pltpu.make_async_copy(extra, ex, e_sem)
     e_copy.start()
-    for h in range(1, heads):
+    for g in range(1, groups):
         for c in range(CHUNKS):
             ks = pl.ds(c * kc, kc)
             for i, w in enumerate((forget_w, value_w)):
                 cp = pltpu.make_async_copy(
-                    w.at[ks, pl.ds(h * HD, HD)],
-                    ws.at[h, ks, pl.ds(i * HD, HD)],
-                    w_sem.at[h, c, i],
+                    w.at[ks, pl.ds(g * wide, wide)],
+                    ws.at[g, ks, pl.ds(i * wide, wide)],
+                    w_sem.at[g, c, i],
                 )
                 cp.start()
-                w_copies[h, c, i] = cp
+                w_copies[g, c, i] = cp
 
     barrier = pltpu.get_barrier_semaphore()
     for k in range(1, m):
@@ -102,24 +104,25 @@
     def lanes(ref, h):
         return ref[pl.ds(h * HD, HD)].reshape(1, HD)
 
-    def matmul(h):
-        tall = rows if h == 0 else rows + PAD
+    def matmul(g):
+        tall = rows if g == 0 else rows + PAD
         for c in range(CHUNKS):
-            if h == 0:
+            if g == 0:
                 for cp in x_copies[c]:
                     cp.wait()
             for i in range(2):
-                w_copies[h, c, i].wait()
+                w_copies[g, c, i].wait()
             ks = pl.ds(c * kc, kc)
-            part = jnp.dot(xs[pl.ds(0, tall), ks], ws[h, ks, :], preferred_element_type=F32)
+            part = jnp.dot(xs[pl.ds(0, tall), ks], ws[g, ks, :], preferred_element_type=F32)
             if c == 0:
-                acc[h % 2, pl.ds(0, tall), :] = part
+                acc[g % 2, pl.ds(0, tall), :] = part
             else:
-                acc[h % 2, pl.ds(0, tall), :] += part
+                acc[g % 2, pl.ds(0, tall), :] += part
 
     t_copies, y_copies, z_copies = {}, {}, {}
 
     def gate(h):
+        g, i = h // GROUP, h % GROUP
         opening = 1.0 - lanes(lower, h)
         at = lax.broadcasted_iota(jnp.int32, (span, HD), 0)
 
@@ -130,8 +133,8 @@
 
         for s in range(seqs):
             block = pl.ds(s * span, span)
-            pre = acc[h % 2, block, pl.ds(0, HD)].astype(BF16).astype(F32)
-            values = acc[h % 2, block, pl.ds(HD, HD)].astype(BF16)
+            pre = acc[g % 2, block, pl.ds(i * HD, HD)].astype(BF16).astype(F32)
+            values = acc[g % 2, block, pl.ds(wide + i * HD, HD)].astype(BF16)
             key = opening / (1.0 + jnp.exp(pre))
             keep = (1.0 - key) * jnp.exp(ex[s, :, pl.ds(h * HD, HD)])
             after = later(keep, 1)
@@ -140,7 +143,7 @@
                 after = after * later(after, k)
                 k *= 2
             weighted = (key * after).astype(BF16)
-            tb[h, me, pl.ds(s, 1), :] = after[0:1] * keep[0:1]
+            tb[g, me, i, pl.ds(s, 1), :] = after[0:1] * keep[0:1]
             state = lax.dot_general(
                 weighted, values, (((0,), (0,)), ((), ())), preferred_element_type=F32
             )
@@ -148,11 +151,15 @@
                 for y in range(near):
                     lo = (f * near + y) * share
                     bs[h, y, f, s] = state[lo : lo + share]
-        t_copies[h] = [
-            send(tb.at[h, me], tb.at[h, me], t_send.at[h, k], t_recv.at[h, k],
+
+    def send_totals(g):
+        t_copies[g] = [
+            send(tb.at[g, me], tb.at[g, me], t_send.at[g, k], t_recv.at[g, k],
                  {"sp": lax.rem(me + k, n)})
             for k in range(1, n)
         ]
+
+    def send_near(h):
         y_copies[h] = []
         for k in range(1, near):
             y = lax.rem(my_near + k, near)
@@ -164,12 +171,10 @@
     def scale_after(h, block):
         total = jnp.ones((seqs, HD), F32)
         for b in range(n):
-            total = total * jnp.where(b > block, tb[h, b], 1.0)
+            total = total * jnp.where(b > block, tb[h // GROUP, b, h % GROUP], 1.0)
         return total
 
     def combine(h):
-        for cp in t_copies[h]:
-            cp.wait_recv()
         sources = [lax.rem(my_near + near - k, near) for k in range(near)]
         scales = [scale_after(h, my_far * near + y) for y in sources]
         fill = HD - near * seqs
@@ -206,8 +211,9 @@
             state_out[h, s] = total.astype(BF16)
 
     def token_terms(h, block):
-        new_pre = block[0:seqs, 0:HD].astype(BF16).astype(F32)
-        new_value = block[0:seqs, HD : 2 * HD].astype(BF16).astype(F32)
+        lo = h % GROUP * HD
+        new_pre = block[0:seqs, lo : lo + HD].astype(BF16).astype(F32)
+        new_value = block[0:seqs, wide + lo : wide + lo + HD].astype(BF16).astype(F32)
         new_key = (1.0 - lanes(lower, h)) / (1.0 + jnp.exp(new_pre))
         q = query[:, pl.ds(h * HD, HD)].astype(F32)
         q = q / (1.0 + jnp.exp(-q))
@@ -225,36 +231,60 @@
                     total += bs[h, y, f, s] * col[lo : lo + share, s : s + 1]
             rp[me, h, pl.ds(s, 1), :] = jnp.sum(total, axis=0, keepdims=True)
 
-    e_waited = False
-    for h in range(heads):
-        if h == 1:
-            for cp in tok_copies:
-                cp.wait_recv()
-            xs[pl.ds(rows, PAD), :] = jnp.zeros((PAD, depth), BF16)
-            for c in range(m):
-                xs[pl.ds(rows, seqs), pl.ds(c * tk, tk)] = toks[c]
-        matmul(h)
-        if not e_waited:
+    def take_tokens():
+        for cp in tok_copies:
+            cp.wait_recv()
+        xs[pl.ds(rows, PAD), :] = jnp.zeros((PAD, depth), BF16)
+        for c in range(m):
+            xs[pl.ds(rows, seqs), pl.ds(c * tk, tk)] = toks[c]
+
+    def take_totals(g):
+        for cp in t_copies[g]:
+            cp.wait_recv()
+
+    def members(g):
+        return range(g * GROUP, (g + 1) * GROUP)
+
+    for g in range(groups):
+        if g == 1:
+            take_tokens()
+        matmul(g)
+        if g == 0:
             e_copy.wait()
-            e_waited = True
-        gate(h)
-        if h >= 1:
-            token_terms(h, acc[h % 2, pl.ds(rows, PAD), :])
-            combine(h - 1)
-        if h >= 2:
-            finish(h - 2)
+        for h in members(g):
+            gate(h)
+        send_totals(g)
+        for h in members(g):
+            send_near(h)
+        if g >= 1:
+            for h in members(g):
+                token_terms(h, acc[g % 2, pl.ds(rows, PAD), :])
+            take_totals(g - 1)
+            for h in members(g - 1):
+                combine(h)
+        if g >= 2:
+            for h in members(g - 2):
+                finish(h)
+    if groups == 1:
+        take_tokens()
     first = jnp.dot(xs[pl.ds(rows, PAD), :], ws[0], preferred_element_type=F32)
-    token_terms(0, first)
-    for h in range(heads - 1):
+    for h in members(0):
+        token_terms(h, first)
+    last = groups - 1
+    for h in range(last * GROUP):
         read_part(h)
-    combine(heads - 1)
-    read_part(heads - 1)
+    take_totals(last)
+    for h in members(last):
+        read_part(h)
     r_copies = [
         send(rp.at[me], rp.at[me], r_send.at[k], r_recv.at[k], {"sp": lax.rem(me + k, n)})
         for k in range(1, n)
     ]
-    if heads > 1:
-        finish(heads - 2)
+    for h in members(last):
+        combine(h)
+    if groups > 1:
+        for h in members(last - 1):
+            finish(h)
     for cp in r_copies:
         cp.wait_recv()
     for h in range(heads):
@@ -264,7 +294,8 @@
         mean = jnp.mean(raw * raw, axis=1, keepdims=True)
         normed = raw * lax.rsqrt(mean + 1e-6) * lanes(gain, 0)
         read_out[:, pl.ds(h * HD, HD)] = normed.astype(BF16)
-    finish(heads - 1)
+    for h in members(last):
+        finish(h)
     for cp in sends:
         cp.wait_send()
 
@@ -274,6 +305,7 @@
     rows = seqs * span
     width = forget_w.shape[1]
     heads = width // HD
+    groups = heads // GROUP
     share = HD // n
     near = near_size(n)
     far = n // near
@@ -290,26 +322,26 @@
         out_specs=(vmem, vmem),
         scratch_shapes=[
             pltpu.VMEM((rows + PAD, depth), BF16),
-            pltpu.VMEM((heads, depth, 2 * HD), BF16),
+            pltpu.VMEM((groups, depth, 2 * GROUP * HD), BF16),
             pltpu.VMEM((seqs, span, width), F32),
-            pltpu.VMEM((2, rows + PAD, 2 * HD), F32),
+            pltpu.VMEM((2, rows + PAD, 2 * GROUP * HD), F32),
             pltpu.VMEM((m, seqs, token.shape[1]), BF16),
             pltpu.VMEM((heads, near, far, seqs, share, HD), F32),
             pltpu.VMEM((heads, near - 1, far, seqs, share, HD), F32),
             pltpu.VMEM((heads, far, seqs, share, HD), F32),
             pltpu.VMEM((heads, far - 1, seqs, share, HD), F32),
-            pltpu.VMEM((heads, n, seqs, HD), F32),
+            pltpu.VMEM((groups, n, GROUP, seqs, HD), F32),
             pltpu.VMEM((n, heads, seqs, HD), F32),
             pltpu.VMEM((heads, near, far, share, HD), F32),
             pltpu.VMEM((heads, seqs, HD), F32),
             pltpu.VMEM((heads, seqs, HD), F32),
             dma((CHUNKS, seqs)),
-            dma((heads, CHUNKS, 2)),
+            dma((groups, CHUNKS, 2)),
             dma,
             dma((m,)),
             dma((m,)),
-            dma((heads, n)),
-            dma((heads, n)),
+            dma((groups, n)),
+            dma((groups, n)),
             dma((heads, near - 1)),
             dma((heads, near - 1)),
             dma((heads, far - 1)),

time: 39.8 us -> 35.9 us (0.902)
  Pallas kernels: 36.1 us -> 32.3 us
    pallas_call x1, Pallas kernels: 36.1 us -> 32.3 us  [local(): pl.pallas_call(functools.partial(kernel, n, m, near), out_shape=(jax.Shap...]
where the time goes in v2:
time: 35.9 us; the launch traced here: 35.7 us
  Pallas kernels  32.3 us (90%)
  local copies, waits for them, and re-layouts  2.77 us (8%)
  between operations  0.64 us (2%)
    pallas_call x1, Pallas kernels, local(): pl.pallas_call(functools.partial(kernel, n, m, near), out_shape=(jax.Shap...  32.3 us
    unnamed x2, local copies, waits for them, and re-layouts  2.77 us

profile of v2, /device:TPU:0, one launch (start us, length us, event | category | flops | bytes accessed | tf_op | source)
XLA Modules:
  0.0 35.7 jit_solution(9060329826257869827)
XLA Ops:
  0.6 32.3 %shard_map.95 = (bf16[4,4,16,128]{3,2,1,0:T(8,128)(2,1)}, bf16[4,512]{1,0:T(4,128)(2,1)}) custom-call(bf16[4,192,4096]{2,1,0:T(8,128)(2,1)} %prompt.1, bf16[4096,512]{1,0:T(8,128)(2,1)} %forget_w.1, bf16[4096,512]{1,0:T(8,128)(2,1)} %value_w.1, f32[512]{0:T(512)} %lower.1, f32[4,192,512]{2,1,0:T(8,128)} %extra.1, bf16[4,1024]{1,0:T(4,128)(2,1)} %token_.1, ...), custom_call_target="tpu_custom_call" | custom-call | tf_op jit(solution)/shard_map/pallas_call | solution.py:315
  32.9 1.5 %copy.10 = bf16[16,4,4,128]{3,2,1,0:T(4,128)(2,1)} copy(bf16[16,4,4,128]{3,0,2,1:T(8,128)(2,1)} %bitcast.1) | data formatting | bytes 131072
  34.4 1.3 %copy.12 = bf16[4,512]{1,0:T(4,128)(2,1)} copy(bf16[4,512]{1,0:T(4,128)(2,1)} %get-tuple-element.11) | data formatting | bytes 8192
